TPU v7x, 32 devices: a whole 2x2x4 slice. The times are simulated.
32 devices in a mesh: sp: 4 (over z), dp: 8 (over y, x, core).
Axes of the slice: x: 2, y: 2, z: 4, core: 2. Of those that a mesh axis runs over, the one named last changes fastest.
Arguments:
- queries: bfloat16 [8, 512, 1024], P('dp', 'sp'), may hold values from -300 to 300
- keys: bfloat16 [8, 512, 1024], P('dp', 'sp'), may hold values from -7 to 7
- values: bfloat16 [8, 512, 1024], P('dp', 'sp'), may hold values from -6 to 6
- cum_gates: float32 [8, 16, 512], P('dp', 'sp'), may hold values from -67 to 0, as said below
- out_weight: bfloat16 [1024, 2048], P(None, 'dp'), may hold values from -0.1875 to 0.1875
Outputs:
- mixed: bfloat16 [8, 512, 2048], P('dp', 'sp')
Inputs may be any that keep to these rules, and one draw needn't show every extreme that they name: `cum_gates`: never rises along positions.
All inputs are finite; a program needn't handle non-finite values.
Results may differ from a plain program's by a relative error of at most 0.011.
Values may be sent and summed in bfloat16 or wider, within the bound.
A program may use at most 64 MiB of HBM per device.

v0:
```python
import jax
import jax.numpy as jnp
from jax import lax
from jax.sharding import PartitionSpec as P


def attend_heads(query_loc, key_loc, value_loc, cum_loc):
    length = query_loc.shape[0]
    head_count = cum_loc.shape[0]
    head_size = query_loc.shape[1] // head_count
    query_heads = query_loc.reshape(length, head_count, head_size).transpose(1, 0, 2)
    key_heads = key_loc.reshape(length, head_count, head_size).transpose(1, 0, 2)
    value_heads = value_loc.reshape(length, head_count, head_size).transpose(1, 0, 2)
    block_rows = min(512, length)
    block_count = length // block_rows
    query_blocks = query_heads.reshape(head_count, block_count, block_rows, head_size).transpose(
        1, 0, 2, 3
    )
    cum_blocks = cum_loc.reshape(head_count, block_count, block_rows).transpose(1, 0, 2)
    key_pos = jnp.arange(length)
    score_scale = head_size ** (-0.5)

    def one_block(packed):
        query_block, cum_block, block_index = packed
        scores = (
            jnp.einsum("hqd,hkd->hqk", query_block, key_heads, preferred_element_type=jnp.float32)
            * score_scale
        )
        scores = scores + cum_block[:, :, None] - cum_loc[:, None, :]
        query_pos = block_index * block_rows + jnp.arange(block_rows)
        scores = jnp.where(key_pos[None, :] <= query_pos[:, None], scores, -jnp.inf)
        row_max = jnp.max(scores, axis=-1, keepdims=True)
        expon = jnp.exp(scores - row_max)
        weights = (expon / jnp.sum(expon, axis=-1, keepdims=True)).astype(jnp.bfloat16)
        return jnp.einsum(
            "hqk,hkd->hqd", weights, value_heads, preferred_element_type=jnp.float32
        ).astype(jnp.bfloat16)

    results = lax.map(one_block, (query_blocks, cum_blocks, jnp.arange(block_count)))
    return results.transpose(0, 2, 1, 3).reshape(length, head_count * head_size)


def shards(queries, keys, values, cum_gates, out_weight):
    query_loc, key_loc, value_loc = (
        lax.all_to_all(queries[0], "sp", split_axis=1, concat_axis=0, tiled=True),
        lax.all_to_all(keys[0], "sp", split_axis=1, concat_axis=0, tiled=True),
        lax.all_to_all(values[0], "sp", split_axis=1, concat_axis=0, tiled=True),
    )
    head_out = attend_heads(query_loc, key_loc, value_loc, cum_gates[0])
    token_rows = lax.all_to_all(head_out, "sp", split_axis=0, concat_axis=1, tiled=True)
    mixed_rows = jnp.dot(
        token_rows,
        lax.all_gather(out_weight, "dp", axis=1, tiled=True),
        preferred_element_type=jnp.float32,
    )
    return mixed_rows.astype(jnp.bfloat16)[None]


def solution(mesh):
    in_specs = (
        P("dp", "sp", None),
        P("dp", "sp", None),
        P("dp", "sp", None),
        P("dp", "sp", None),
        P(None, "dp"),
    )
    out_specs = P("dp", "sp", None)
    return jax.shard_map(shards, mesh=mesh, in_specs=in_specs, out_specs=out_specs, check_vma=False)
```

profile of v0, /device:TPU:0, one launch (start us, length us, event | category | flops | bytes accessed | tf_op | source)
XLA Modules:
  0.0 70.6 jit_solution(15589185391512869940)
XLA Ops:
  6.5 0.0 copy-start
  6.5 0.0 all-gather.2.cloned.1.call-start
  6.5 0.7 %all-gather.2.cloned.1.call-update = ((bf16[1024,256]{1,0:T(8,128)(2,1)}), bf16[1024,2048]{1,0:T(8,128)(2,1)}) async-update(((), (), s32[]{:S(2)}) %all-gather.2.cloned.1.call-start, bf16[1024,256]{1,0:T(8,128)(2,1)} %param.9) | async-update | bytes 5242904
  7.3 1.8 %copy.15 = bf16[1,128,1024]{1,2,0:T(8,128)(2,1)} copy(bf16[1,128,1024]{2,1,0:T(8,128)(2,1)} %param.5) | data formatting | bytes 524288 | tf_op args[0]
  9.0 6.3 %all-to-all-start = ((bf16[128,4,256]{0,2,1:T(8,128)(2,1)}), bf16[128,4,256]{0,2,1:T(8,128)(2,1)S(1)}, u32[]{:S(2)}, u32[]{:S(2)}) async-start(bf16[128,4,256]{0,2,1:T(8,128)(2,1)} %bitcast), calls=%async_computation | async-start | bytes 524288 | tf_op jit(solution)/shard_map/all_to_all | solution.py:45
  15.4 1.8 %copy.17 = bf16[1,128,1024]{1,2,0:T(8,128)(2,1)} copy(bf16[1,128,1024]{2,1,0:T(8,128)(2,1)} %param.6) | data formatting | bytes 524288 | tf_op args[1]
  17.2 7.1 %all-to-all-done = bf16[128,4,256]{0,2,1:T(8,128)(2,1)S(1)} async-done(((bf16[128,4,256]{0,2,1:T(8,128)(2,1)}), bf16[128,4,256]{0,2,1:T(8,128)(2,1)S(1)}, u32[]{:S(2)}, u32[]{:S(2)}) %all-to-all-start) | async-done | bytes 262176 | tf_op jit(solution)/shard_map/all_to_all | solution.py:45
  24.3 3.4 %all-to-all-start.1 = ((bf16[128,4,256]{0,2,1:T(8,128)(2,1)}), bf16[128,4,256]{0,2,1:T(8,128)(2,1)S(1)}, u32[]{:S(2)}, u32[]{:S(2)}) async-start(bf16[128,4,256]{0,2,1:T(8,128)(2,1)} %bitcast.3), calls=%async_computation.1 | async-start | bytes 524288 | tf_op jit(solution)/shard_map/all_to_all | solution.py:46
  27.7 1.8 %copy.19 = bf16[1,128,1024]{1,2,0:T(8,128)(2,1)} copy(bf16[1,128,1024]{2,1,0:T(8,128)(2,1)} %param.7) | data formatting | bytes 524288 | tf_op args[2]
  29.5 5.2 %all-to-all-done.1 = bf16[128,4,256]{0,2,1:T(8,128)(2,1)S(1)} async-done(((bf16[128,4,256]{0,2,1:T(8,128)(2,1)}), bf16[128,4,256]{0,2,1:T(8,128)(2,1)S(1)}, u32[]{:S(2)}, u32[]{:S(2)}) %all-to-all-start.1) | async-done | bytes 262176 | tf_op jit(solution)/shard_map/all_to_all | solution.py:46
  34.7 3.4 %all-to-all-start.2 = ((bf16[128,4,256]{0,2,1:T(8,128)(2,1)}), bf16[128,4,256]{0,2,1:T(8,128)(2,1)S(1)}, u32[]{:S(2)}, u32[]{:S(2)}) async-start(bf16[128,4,256]{0,2,1:T(8,128)(2,1)} %bitcast.7), calls=%async_computation.2 | async-start | bytes 524288 | tf_op jit(solution)/shard_map/all_to_all | solution.py:47
  38.1 0.1 iota_compare_fusion
  38.2 0.2 copy.16
  38.4 0.1 reshape.37
  38.5 0.2 copy.18
  38.8 0.1 reshape.38
  38.9 6.0 %all-to-all-done.2 = bf16[128,4,256]{0,2,1:T(8,128)(2,1)S(1)} async-done(((bf16[128,4,256]{0,2,1:T(8,128)(2,1)}), bf16[128,4,256]{0,2,1:T(8,128)(2,1)S(1)}, u32[]{:S(2)}, u32[]{:S(2)}) %all-to-all-start.2) | async-done | bytes 262176 | tf_op jit(solution)/shard_map/all_to_all | solution.py:47
  44.9 0.2 copy.20
  45.1 0.1 reshape.39
  45.2 0.0 copy-done
  45.2 2.2 %fusion.37 = f32[4,512]{1,0:T(4,128)S(1)} fusion(f32[4,512]{1,0:T(4,128)S(1)} %bitcast.61, pred[512,512]{0,1:T(8,128)(4,1)S(1)} %iota_compare_fusion, bf16[512,4,64]{0,2,1:T(8,128)(2,1)S(1)} %reshape.38, bf16[512,4,64]{0,2,1:T(8,128)(2,1)S(1)} %reshape.37), kind=kOutput, calls=%fused_computation.27 | convolution fusion | flops 140509696 | bytes 802816 | tf_op jit(solution)/shard_map/while/body/eval_jaxpr/sub | solution.py:33
  47.4 2.2 %fusion.10 = bf16[1,512,4,64]{1,3,2,0:T(8,128)(2,1)S(1)} fusion(f32[4,512]{1,0:T(4,128)S(1)} %fusion.37, bf16[512,4,64]{0,2,1:T(8,128)(2,1)S(1)} %reshape.39, f32[4,512]{1,0:T(4,128)S(1)} %bitcast.62, pred[512,512]{0,1:T(8,128)(4,1)S(1)} %iota_compare_fusion, bf16[512,4,64]{0,2,1:T(8,128)(2,1)S(1)} %reshape.38, bf16[512,4,64]{0,2,1:T(8,128)(2,1)S(1)} %reshape.37), kind=kOutput, calls=%fused_computation.14 | convolution fusion | flops 275909120 | bytes 1327104 | tf_op jit(solution)/shard_map/while/body/eval_jaxpr/hqk,hkd->hqd/dot_general | solution.py:35
  49.6 0.1 all_to_all.59
  49.7 10.4 %all_to_all.67 = bf16[4,128,256]{1,2,0:T(8,128)(2,1)S(1)} all-to-all(bf16[4,128,256]{1,2,0:T(8,128)(2,1)S(1)} %copy.22), channel_id=1, replica_groups=mesh['sp'=4,'dp'=8] {'sp'}, dimensions={0} | all-to-all | bytes 524288 | tf_op jit(solution)/shard_map/all_to_all | solution.py:50
  60.1 0.0 all-gather.2.cloned.1.call-done
  60.1 3.7 %fusion.2 = bf16[1,128,2048]{2,1,0:T(8,128)(2,1)} fusion(bf16[128,1024]{0,1:T(8,128)(2,1)S(1)} %bitcast.57, bf16[1024,2048]{1,0:T(8,128)(2,1)} %all-gather.2.cloned.1.call-done), kind=kOutput, calls=%fused_computation.6 | convolution fusion | flops 537133056 | bytes 4980736 | tf_op jit(solution)/shard_map/dot_general | solution.py:51
  (1 shorter events, 0.0 us)
Async XLA Ops:
  6.5 38.7 %copy-start = (f32[1,4,512]{2,1,0:T(4,128)S(1)}, f32[1,4,512]{2,1,0:T(4,128)}, u32[]{:S(2)}) copy-start(f32[1,4,512]{2,1,0:T(4,128)} %param.8) | copy-start | bytes 24580
  6.5 53.5 %all-gather.2.cloned.1.call-start = ((), (), s32[]{:S(2)}) async-start(), calls=%async_computation.4 | async-start | bytes 4718592 | tf_op jit(solution)/shard_map/all_gather | solution.py:53
  9.0 15.3 %all-to-all-start = ((bf16[128,4,256]{0,2,1:T(8,128)(2,1)}), bf16[128,4,256]{0,2,1:T(8,128)(2,1)S(1)}, u32[]{:S(2)}, u32[]{:S(2)}) async-start(bf16[128,4,256]{0,2,1:T(8,128)(2,1)} %bitcast), calls=%async_computation | async-start | bytes 524288 | tf_op jit(solution)/shard_map/all_to_all | solution.py:45
  24.3 10.4 %all-to-all-start.1 = ((bf16[128,4,256]{0,2,1:T(8,128)(2,1)}), bf16[128,4,256]{0,2,1:T(8,128)(2,1)S(1)}, u32[]{:S(2)}, u32[]{:S(2)}) async-start(bf16[128,4,256]{0,2,1:T(8,128)(2,1)} %bitcast.3), calls=%async_computation.1 | async-start | bytes 524288 | tf_op jit(solution)/shard_map/all_to_all | solution.py:46
  34.7 10.2 %all-to-all-start.2 = ((bf16[128,4,256]{0,2,1:T(8,128)(2,1)}), bf16[128,4,256]{0,2,1:T(8,128)(2,1)S(1)}, u32[]{:S(2)}, u32[]{:S(2)}) async-start(bf16[128,4,256]{0,2,1:T(8,128)(2,1)} %bitcast.7), calls=%async_computation.2 | async-start | bytes 524288 | tf_op jit(solution)/shard_map/all_to_all | solution.py:47
Sparse Core Ops, SparseCore 0:
  9.2 40.0 all-gather.1
where the time goes:
time: 71.1 us; the launch traced here: 70.6 us
  waiting for transfers between devices  19.1 us (27%)
  between operations  13.5 us (19%)
  starting transfers between devices  13.2 us (19%)
  blocking collectives  10.4 us (15%)
  matrix products  8.1 us (11%)
  local copies, waits for them, and re-layouts  6.39 us (9%)
    all_to_all x1, blocking collectives, shards(): lax.all_to_all(head_out, 'sp', split_axis=0, concat_axis=1, tiled=True)  10.4 us
    all_to_all x1, waiting for transfers between devices, shards(): lax.all_to_all(queries[0], 'sp', split_axis=1, concat_axis=0, tiled=True)  7.12 us
    all_to_all x1, starting transfers between devices, shards(): lax.all_to_all(queries[0], 'sp', split_axis=1, concat_axis=0, tiled=True)  6.35 us
    all_to_all x1, waiting for transfers between devices, shards(): lax.all_to_all(values[0], 'sp', split_axis=1, concat_axis=0, tiled=True)  6.01 us
    unnamed x5, local copies, waits for them, and re-layouts  5.36 us
    all_to_all x1, waiting for transfers between devices, shards(): lax.all_to_all(keys[0], 'sp', split_axis=1, concat_axis=0, tiled=True)  5.21 us
    dot_general x1, matrix products, shards(): jnp.dot(token_rows, lax.all_gather(out_weight, 'dp', axis=1, tiled=True),...  3.72 us
    all_to_all x1, starting transfers between devices, shards(): lax.all_to_all(keys[0], 'sp', split_axis=1, concat_axis=0, tiled=True)  3.41 us
  transfers between devices with their start and end apart: 4, of which 3 were waited for; matrix products, arithmetic and copies ran while one was open for 15% of the time, Pallas kernels for 0%

commit v1 on v0

--- a/solution.py
+++ b/solution.py
@@ -2,6 +2,16 @@
 import jax.numpy as jnp
 from jax import lax
 from jax.sharding import PartitionSpec as P
+
+fill_chains = lambda view, across, axis_k, where_dim: jnp.concatenate(
+    jax.lax.all_to_all(
+        jnp.stack(jnp.split(view, jax.lax.psum(1, axis_name=across), axis=axis_k), axis=0),
+        axis_name=across,
+        split_axis=0,
+        concat_axis=0,
+    ),
+    axis=where_dim,
+)
 
 
 def attend_heads(query_loc, key_loc, value_loc, cum_loc):
@@ -44,7 +54,7 @@
     query_loc, key_loc, value_loc = (
         lax.all_to_all(queries[0], "sp", split_axis=1, concat_axis=0, tiled=True),
         lax.all_to_all(keys[0], "sp", split_axis=1, concat_axis=0, tiled=True),
-        lax.all_to_all(values[0], "sp", split_axis=1, concat_axis=0, tiled=True),
+        fill_chains(values[0], "sp", 1, 0),
     )
     head_out = attend_heads(query_loc, key_loc, value_loc, cum_gates[0])
     token_rows = lax.all_to_all(head_out, "sp", split_axis=0, concat_axis=1, tiled=True)

time: 71.1 us -> 71.1 us (level)
  local copies, waits for them, and re-layouts: 6.39 us -> 5.54 us
  other arithmetic: 0.08 us -> 0.82 us
    all_to_all x1, starting transfers between devices: 3.4 us -> 6.35 us  [jax.lax.all_to_all(jnp.stack(jnp.split(view, jax.lax.psum(1, axis_name=ac...]
    all_to_all x1, starting transfers between devices: 6.35 us -> 3.4 us  [shards(): lax.all_to_all(queries[0], 'sp', split_axis=1, concat_axis=0, tiled=True)]
    all_to_all x1, waiting for transfers between devices: 7.12 us -> 5.21 us  [shards(): lax.all_to_all(queries[0], 'sp', split_axis=1, concat_axis=0, tiled=True)]
    unnamed x5 -> x4, local copies, waits for them, and re-layouts: 5.36 us -> 3.57 us
    all_to_all x1, waiting for transfers between devices: 6.01 us -> 7.13 us  [jax.lax.all_to_all(jnp.stack(jnp.split(view, jax.lax.psum(1, axis_name=ac...]
    another operation x0 -> x2, local copies, waits for them, and re-layouts: none -> 1.06 us  [the longest x1 0.96 us: jnp.stack(jnp.split(view, jax.lax.psum(1, axis_name=across), axis=axis_k)...]
    all_to_all x1, waiting for transfers between devices: 5.21 us -> 6.03 us  [shards(): lax.all_to_all(keys[0], 'sp', split_axis=1, concat_axis=0, tiled=True)]
    another operation x0 -> x1, other arithmetic: none -> 0.74 us  [jnp.stack(jnp.split(view, jax.lax.psum(1, axis_name=across), axis=axis_k)...]
where the time goes in v1:
time: 71.1 us; the launch traced here: 70.5 us
  waiting for transfers between devices  19.1 us (27%)
  between operations  13.5 us (19%)
  starting transfers between devices  13.2 us (19%)
  blocking collectives  10.4 us (15%)
  matrix products  8.1 us (11%)
  local copies, waits for them, and re-layouts  5.54 us (8%)
  other arithmetic  0.82 us (1%)
    all_to_all x1, blocking collectives, shards(): lax.all_to_all(head_out, 'sp', split_axis=0, concat_axis=1, tiled=True)  10.4 us
    all_to_all x1, waiting for transfers between devices, jax.lax.all_to_all(jnp.stack(jnp.split(view, jax.lax.psum(1, axis_name=ac...  7.13 us
    all_to_all x1, starting transfers between devices, jax.lax.all_to_all(jnp.stack(jnp.split(view, jax.lax.psum(1, axis_name=ac...  6.35 us
    all_to_all x1, waiting for transfers between devices, shards(): lax.all_to_all(keys[0], 'sp', split_axis=1, concat_axis=0, tiled=True)  6.03 us
    all_to_all x1, waiting for transfers between devices, shards(): lax.all_to_all(queries[0], 'sp', split_axis=1, concat_axis=0, tiled=True)  5.21 us
    dot_general x1, matrix products, shards(): jnp.dot(token_rows, lax.all_gather(out_weight, 'dp', axis=1, tiled=True),...  3.73 us
    unnamed x4, local copies, waits for them, and re-layouts  3.57 us
    all_to_all x1, starting transfers between devices, shards(): lax.all_to_all(keys[0], 'sp', split_axis=1, concat_axis=0, tiled=True)  3.41 us
  transfers between devices with their start and end apart: 4, of which 3 were waited for; matrix products, arithmetic and copies ran while one was open for 15% of the time, Pallas kernels for 0%

profile of v1, /device:TPU:0, one launch (start us, length us, event | category | flops | bytes accessed | tf_op | source)
XLA Modules:
  0.0 70.5 jit_solution(1021142222102623833)
XLA Ops:
  6.5 0.0 copy-start
  6.5 0.0 all-gather.2.cloned.1.call-start
  6.5 0.7 %all-gather.2.cloned.1.call-update = ((bf16[1024,256]{1,0:T(8,128)(2,1)}), bf16[1024,2048]{1,0:T(8,128)(2,1)}) async-update(((), (), s32[]{:S(2)}) %all-gather.2.cloned.1.call-start, bf16[1024,256]{1,0:T(8,128)(2,1)} %param.9) | async-update | bytes 5242904
  7.3 1.0 %slice_bitcast_fusion.3 = (bf16[1,128,256]{2,1,0:T(8,128)(2,1)S(1)}, bf16[1,128,256]{2,1,0:T(8,128)(2,1)S(1)}, bf16[1,128,256]{2,1,0:T(8,128)(2,1)S(1)}, bf16[1,128,256]{2,1,0:T(8,128)(2,1)S(1)}) fusion(bf16[128,1024]{1,0:T(8,128)(2,1)} %bitcast.67), kind=kLoop, calls=%fused_computation.27 | loop fusion | bytes 524288 | tf_op jit(solution)/shard_map/stack | solution.py:8
  8.2 0.7 %pad_maximum_fusion = bf16[4,128,256]{2,1,0:T(8,128)(2,1)} fusion(bf16[1,128,256]{2,1,0:T(8,128)(2,1)S(1)} %get-tuple-element.18, bf16[1,128,256]{2,1,0:T(8,128)(2,1)S(1)} %get-tuple-element.19, bf16[1,128,256]{2,1,0:T(8,128)(2,1)S(1)} %get-tuple-element.20, bf16[1,128,256]{2,1,0:T(8,128)(2,1)S(1)} %get-tuple-element.17), kind=kLoop, calls=%fused_computation.17 | loop fusion | flops 393216 | bytes 524288 | tf_op jit(solution)/shard_map/stack | solution.py:8
  9.0 6.3 %all-to-all-start.2 = ((bf16[4,128,256]{2,1,0:T(8,128)(2,1)}), bf16[4,128,256]{2,1,0:T(8,128)(2,1)S(1)}, u32[]{:S(2)}, u32[]{:S(2)}) async-start(bf16[4,128,256]{2,1,0:T(8,128)(2,1)} %pad_maximum_fusion), calls=%async_computation.2 | async-start | bytes 524288 | tf_op jit(solution)/shard_map/all_to_all | solution.py:7
  15.3 1.8 %copy.15 = bf16[1,128,1024]{1,2,0:T(8,128)(2,1)} copy(bf16[1,128,1024]{2,1,0:T(8,128)(2,1)} %param.5) | data formatting | bytes 524288 | tf_op args[0]
  17.1 7.1 %all-to-all-done.2 = bf16[4,128,256]{2,1,0:T(8,128)(2,1)S(1)} async-done(((bf16[4,128,256]{2,1,0:T(8,128)(2,1)}), bf16[4,128,256]{2,1,0:T(8,128)(2,1)S(1)}, u32[]{:S(2)}, u32[]{:S(2)}) %all-to-all-start.2) | async-done | bytes 262176 | tf_op jit(solution)/shard_map/all_to_all | solution.py:7
  24.2 3.4 %all-to-all-start = ((bf16[128,4,256]{0,2,1:T(8,128)(2,1)}), bf16[128,4,256]{0,2,1:T(8,128)(2,1)S(1)}, u32[]{:S(2)}, u32[]{:S(2)}) async-start(bf16[128,4,256]{0,2,1:T(8,128)(2,1)} %bitcast), calls=%async_computation | async-start | bytes 524288 | tf_op jit(solution)/shard_map/all_to_all | solution.py:55
  27.6 1.8 %copy.17 = bf16[1,128,1024]{1,2,0:T(8,128)(2,1)} copy(bf16[1,128,1024]{2,1,0:T(8,128)(2,1)} %param.6) | data formatting | bytes 524288 | tf_op args[1]
  29.4 5.2 %all-to-all-done = bf16[128,4,256]{0,2,1:T(8,128)(2,1)S(1)} async-done(((bf16[128,4,256]{0,2,1:T(8,128)(2,1)}), bf16[128,4,256]{0,2,1:T(8,128)(2,1)S(1)}, u32[]{:S(2)}, u32[]{:S(2)}) %all-to-all-start) | async-done | bytes 262176 | tf_op jit(solution)/shard_map/all_to_all | solution.py:55
  34.6 3.4 %all-to-all-start.1 = ((bf16[128,4,256]{0,2,1:T(8,128)(2,1)}), bf16[128,4,256]{0,2,1:T(8,128)(2,1)S(1)}, u32[]{:S(2)}, u32[]{:S(2)}) async-start(bf16[128,4,256]{0,2,1:T(8,128)(2,1)} %bitcast.3), calls=%async_computation.1 | async-start | bytes 524288 | tf_op jit(solution)/shard_map/all_to_all | solution.py:56
  38.0 0.1 iota_compare_fusion
  38.1 0.2 copy.19
  38.3 0.1 reshape_reshape.3
  38.4 0.2 copy.16
  38.6 0.1 reshape.29
  38.8 6.0 %all-to-all-done.1 = bf16[128,4,256]{0,2,1:T(8,128)(2,1)S(1)} async-done(((bf16[128,4,256]{0,2,1:T(8,128)(2,1)}), bf16[128,4,256]{0,2,1:T(8,128)(2,1)S(1)}, u32[]{:S(2)}, u32[]{:S(2)}) %all-to-all-start.1) | async-done | bytes 262176 | tf_op jit(solution)/shard_map/all_to_all | solution.py:56
  44.8 0.2 copy.18
  45.0 0.1 reshape.30
  45.1 0.0 copy-done
  45.1 2.2 %fusion.37 = f32[4,512]{1,0:T(4,128)S(1)} fusion(f32[4,512]{1,0:T(4,128)S(1)} %bitcast.68, pred[512,512]{0,1:T(8,128)(4,1)S(1)} %iota_compare_fusion, bf16[512,4,64]{0,2,1:T(8,128)(2,1)S(1)} %reshape.30, bf16[512,4,64]{0,2,1:T(8,128)(2,1)S(1)} %reshape.29), kind=kOutput, calls=%fused_computation.32 | convolution fusion | flops 140509696 | bytes 802816 | tf_op jit(solution)/shard_map/while/body/eval_jaxpr/sub | solution.py:43
  47.3 2.2 %fusion.10 = bf16[1,512,4,64]{1,3,2,0:T(8,128)(2,1)S(1)} fusion(f32[4,512]{1,0:T(4,128)S(1)} %fusion.37, bf16[512,4,64]{0,2,1:T(8,128)(2,1)S(1)} %reshape_reshape.3, f32[4,512]{1,0:T(4,128)S(1)} %bitcast.69, pred[512,512]{0,1:T(8,128)(4,1)S(1)} %iota_compare_fusion, bf16[512,4,64]{0,2,1:T(8,128)(2,1)S(1)} %reshape.30, bf16[512,4,64]{0,2,1:T(8,128)(2,1)S(1)} %reshape.29), kind=kOutput, calls=%fused_computation.14 | convolution fusion | flops 275909120 | bytes 1327104 | tf_op jit(solution)/shard_map/while/body/eval_jaxpr/hqk,hkd->hqd/dot_general | solution.py:45
  49.5 0.1 all_to_all.48
  49.6 10.4 %all_to_all.56 = bf16[4,128,256]{1,2,0:T(8,128)(2,1)S(1)} all-to-all(bf16[4,128,256]{1,2,0:T(8,128)(2,1)S(1)} %copy.21), channel_id=1, replica_groups=mesh['sp'=4,'dp'=8] {'sp'}, dimensions={0} | all-to-all | bytes 524288 | tf_op jit(solution)/shard_map/all_to_all | solution.py:60
  60.0 0.0 all-gather.2.cloned.1.call-done
  60.0 3.7 %fusion.2 = bf16[1,128,2048]{2,1,0:T(8,128)(2,1)} fusion(bf16[128,1024]{0,1:T(8,128)(2,1)S(1)} %bitcast.64, bf16[1024,2048]{1,0:T(8,128)(2,1)} %all-gather.2.cloned.1.call-done), kind=kOutput, calls=%fused_computation.6 | convolution fusion | flops 537133056 | bytes 4980736 | tf_op jit(solution)/shard_map/dot_general | solution.py:61
  (1 shorter events, 0.0 us)
Async XLA Ops:
  6.5 38.6 %copy-start = (f32[1,4,512]{2,1,0:T(4,128)S(1)}, f32[1,4,512]{2,1,0:T(4,128)}, u32[]{:S(2)}) copy-start(f32[1,4,512]{2,1,0:T(4,128)} %param.8) | copy-start | bytes 24580
  6.5 53.4 %all-gather.2.cloned.1.call-start = ((), (), s32[]{:S(2)}) async-start(), calls=%async_computation.4 | async-start | bytes 4718592 | tf_op jit(solution)/shard_map/all_gather | solution.py:63
  9.0 15.3 %all-to-all-start.2 = ((bf16[4,128,256]{2,1,0:T(8,128)(2,1)}), bf16[4,128,256]{2,1,0:T(8,128)(2,1)S(1)}, u32[]{:S(2)}, u32[]{:S(2)}) async-start(bf16[4,128,256]{2,1,0:T(8,128)(2,1)} %pad_maximum_fusion), calls=%async_computation.2 | async-start | bytes 524288 | tf_op jit(solution)/shard_map/all_to_all | solution.py:7
  24.2 10.4 %all-to-all-start = ((bf16[128,4,256]{0,2,1:T(8,128)(2,1)}), bf16[128,4,256]{0,2,1:T(8,128)(2,1)S(1)}, u32[]{:S(2)}, u32[]{:S(2)}) async-start(bf16[128,4,256]{0,2,1:T(8,128)(2,1)} %bitcast), calls=%async_computation | async-start | bytes 524288 | tf_op jit(solution)/shard_map/all_to_all | solution.py:55
  34.6 10.2 %all-to-all-start.1 = ((bf16[128,4,256]{0,2,1:T(8,128)(2,1)}), bf16[128,4,256]{0,2,1:T(8,128)(2,1)S(1)}, u32[]{:S(2)}, u32[]{:S(2)}) async-start(bf16[128,4,256]{0,2,1:T(8,128)(2,1)} %bitcast.3), calls=%async_computation.1 | async-start | bytes 524288 | tf_op jit(solution)/shard_map/all_to_all | solution.py:56
Sparse Core Ops, SparseCore 0:
  9.2 40.0 all-gather.1
